TPU v7x, 128 devices: a 2x2x16 block of a 8x8x16 slice. The times are simulated.
128 devices in a mesh: grp: 4 (over y, x), tp: 32 (over z, core).
Axes of the slice: x: 2, y: 2, z: 16, core: 2. Of those that a mesh axis runs over, the one named last changes fastest.
The devices are a block of a 8x8x16 slice.
Arguments:
- tokens: bfloat16 [4096, 2048], P('grp', 'tp'), parts along dimension 0, may hold values from -8 to 8
- carried: float32 [2, 2, 32, 64, 4096], P(None, None, 'tp', None, 'grp'), parts along dimension 4, may hold values from -3 to 3
- proj_in: bfloat16 [2, 2048, 512], P(None, None, 'tp'), may hold values from -0.125 to 0.125
- proj_gate: bfloat16 [2, 2048, 512], P(None, None, 'tp'), may hold values from -0.125 to 0.125
- proj_out: bfloat16 [2, 512, 2048], P(None, None, 'tp'), may hold values from -0.5 to 0.5
- norm_params: bfloat16 [2, 2, 2048], P(None, None, 'tp'), may hold values from -0.5 to 2.4
- lambda_re: float32 [2, 32, 64], P(None, 'tp'), may hold values from -1 to -0.05
- lambda_im: float32 [2, 32, 64], P(None, 'tp'), may hold values from -3 to 3
- log_step: float32 [2, 32], P(None, 'tp'), may hold values from -3 to 0
- in_coupling: float32 [2, 2, 32, 64, 16], P(None, None, 'tp'), may hold values from -1 to 1
- out_coupling: float32 [2, 2, 32, 16, 64], P(None, None, 'tp'), may hold values from -1.5 to 1.5
- skip_gain: float32 [2, 512], P(None, 'tp'), may hold values from -4 to 4
Outputs:
- stream_out: bfloat16 [4096, 2048], P('grp', 'tp'), parts along dimension 0
- new_carried: float32 [2, 2, 32, 64, 4096], P(None, None, 'tp', None, 'grp'), parts along dimension 4
There are 4 independent parts, one for each index of `grp`. A program takes and returns all parts, laid end to end along the dimension named above; an argument that names none is the same for every part. Nothing has to cross between parts.
All inputs are finite; a program needn't handle non-finite values.
Results may differ from a plain program's by a relative error of at most 0.015.
Values may be sent and summed in bfloat16 or wider, within the bound.
A program may use at most 64 MiB of HBM per device.

v0:
```python
import jax
import jax.numpy as jnp
from jax import lax
from jax.sharding import Mesh
from jax.sharding import PartitionSpec as P

TP = ("tp_0", "tp_1")


residual_scale = 1.4142135623730951
norm_eps = 1e-05


def gather_turned(arrays, axis, dims):
    turned = [jnp.moveaxis(a, dim, 0) for a, dim in zip(arrays, dims)]
    both = jnp.concatenate([t.reshape(len(t), -1) for t in turned], axis=1)
    out, at, finished = (lax.all_gather(both, axis, axis=0, tiled=True), 0, [])
    for t, dim in zip(turned, dims):
        piece = out[:, at : at + t[0].size].reshape(-1, *t.shape[1:])
        finished.append(jnp.moveaxis(piece, 0, dim))
        at += t[0].size
    return tuple(finished)


def in_order(tiles, dim):
    tiles = jnp.moveaxis(tiles, 0, dim)
    shape = tiles.shape
    return tiles.reshape(*shape[:dim], shape[dim] * shape[dim + 1], *shape[dim + 2 :])


def all_blocks(array, axes, sequence):
    tiles = array
    for k in sequence:
        tiles = lax.all_gather(tiles, axes[k])
    done = sequence[::-1]
    back = [done.index(k) for k in range(len(axes))]
    tiles = tiles.transpose(*back, *range(len(axes), tiles.ndim))
    return tiles.reshape(-1, *array.shape)


def gather_axes(array, axes, sequence, dim):
    return in_order(all_blocks(array, axes, sequence), dim)


def discretize(lam_re, lam_im, log_dt, coupling):
    step_len = jnp.exp(log_dt)[:, None]
    modulus = jnp.exp(lam_re * step_len)
    decay_re = modulus * jnp.cos(lam_im * step_len)
    decay_im = modulus * jnp.sin(lam_im * step_len)
    denominator = lam_re * lam_re + lam_im * lam_im
    shifted = decay_re - 1.0
    coef_re = (shifted * lam_re + decay_im * lam_im) / denominator
    coef_im = (decay_im * lam_re - shifted * lam_im) / denominator
    in_re = coef_re[..., None] * coupling[0] - coef_im[..., None] * coupling[1]
    in_im = coef_re[..., None] * coupling[1] + coef_im[..., None] * coupling[0]
    return (decay_re, decay_im, in_re, in_im)


def recur(drive, gate_pre, states, lam_re, lam_im, log_dt, in_c, output_coupling, skip_connection):
    channel_groups = lam_re.shape[0]
    batch_rows = drive.shape[0]
    drive_expanded = drive.astype(jnp.float32).reshape(batch_rows, channel_groups, -1)
    decay_re, decay_im, in_re, in_im = discretize(lam_re, lam_im, log_dt, in_c)
    push_re = jnp.einsum("bgc,gpc->gpb", drive_expanded, in_re)
    push_im = jnp.einsum("bgc,gpc->gpb", drive_expanded, in_im)
    fresh_real = decay_re[..., None] * states[0] - decay_im[..., None] * states[1] + push_re
    fresh_imaginary = decay_re[..., None] * states[1] + decay_im[..., None] * states[0] + push_im
    readout_rows = (
        jnp.einsum("jyn,jmy->njm", fresh_real, output_coupling[0])
        - jnp.einsum("jyn,jmy->njm", fresh_imaginary, output_coupling[1])
        + skip_connection.reshape(channel_groups, -1) * drive_expanded
    )
    readout_rows = readout_rows.reshape(batch_rows, -1)
    gated = (jax.nn.gelu(readout_rows) * jax.nn.sigmoid(gate_pre.astype(jnp.float32))).astype(
        jnp.bfloat16
    )
    return (gated, jnp.stack([fresh_real, fresh_imaginary]))


def norm_whole(summed, params):
    wide = summed.astype(jnp.float32)
    mean_row = jnp.mean(wide, axis=-1, keepdims=True)
    var_row = jnp.mean(wide * wide, axis=-1, keepdims=True) - mean_row * mean_row
    scaled = (wide - mean_row) * lax.rsqrt(var_row + norm_eps)
    return (scaled * params[0].astype(jnp.float32) + params[1].astype(jnp.float32)).astype(
        jnp.bfloat16
    )


def per_device(
    tokens,
    carried,
    proj_in,
    proj_gate,
    proj_out,
    norm_params,
    lambda_re,
    lambda_im,
    log_step,
    in_coupling,
    out_coupling,
    skip_gain,
):
    layer_count = proj_in.shape[0]
    width_dev = tokens.shape[1]
    out_whole, params_whole = gather_turned((proj_out, norm_params), TP, (2, 2))
    whole_rows = lax.all_gather(tokens, TP, axis=1, tiled=True)
    new_states = []
    for layer_idx in range(layer_count):
        drive = jnp.dot(whole_rows, proj_in[layer_idx], preferred_element_type=jnp.float32).astype(
            jnp.bfloat16
        )
        gate_pre = jnp.dot(
            whole_rows, proj_gate[layer_idx], preferred_element_type=jnp.float32
        ).astype(jnp.bfloat16)
        gated, states = recur(
            drive,
            gate_pre,
            carried[layer_idx],
            lambda_re[layer_idx],
            lambda_im[layer_idx],
            log_step[layer_idx],
            in_coupling[layer_idx],
            out_coupling[layer_idx],
            skip_gain[layer_idx],
        )
        gated_all = gather_axes(gated, TP, (0, 1), 1)
        mixed = jnp.dot(gated_all, out_whole[layer_idx], preferred_element_type=jnp.float32)
        summed = (residual_scale * whole_rows.astype(jnp.float32) + mixed).astype(jnp.bfloat16)
        whole_rows = norm_whole(summed, params_whole[layer_idx])
        new_states.append(states)
    own_cols = lax.dynamic_slice_in_dim(whole_rows, lax.axis_index(TP) * width_dev, width_dev, 1)
    return (own_cols, jnp.stack(new_states))


def solution(mesh):
    finer = Mesh(mesh.devices.reshape(mesh.shape["grp"], 16, 2), ("grp", "tp_0", "tp_1"))
    return jax.shard_map(
        per_device,
        mesh=finer,
        in_specs=(
            P("grp", TP),
            P(None, None, TP, None, "grp"),
            P(None, None, TP),
            P(None, None, TP),
            P(None, None, TP),
            P(None, None, TP),
            P(None, TP, None),
            P(None, TP, None),
            P(None, TP),
            P(None, None, TP, None, None),
            P(None, None, TP, None, None),
            P(None, TP),
        ),
        out_specs=(P("grp", TP), P(None, None, TP, None, "grp")),
        check_vma=False,
    )
```

profile of v0, /device:TPU:69, one launch (start us, length us, event | category | flops | bytes accessed | tf_op | source)
XLA Modules:
  0.0 249.1 jit_solution(6978325671678053711)
XLA Ops:
  7.2 0.1 all-gather.9.cloned.1.call-start
  7.3 0.7 all-gather.9.cloned.1.call-update
  8.0 0.1 all-gather.11.cloned.1.call-start
  8.1 0.8 copy.43
  8.9 0.9 copy.54
  9.8 0.7 pad_maximum_fusion
  10.5 0.1 all-gather.13.cloned.1.call-start
  10.6 1.3 fusion.103
  13.3 0.8 slice_bitcast_fusion.4
  14.0 0.7 fusion.91
  14.8 0.8 fusion.97
  15.5 0.7 fusion.100
  16.2 71.2 %all-gather.9.cloned.1.call-done = bf16[1024,2048]{0,1:T(8,128)(2,1)} async-done(((bf16[1024,64]{0,1:T(8,128)(2,1)}), bf16[1024,2048]{0,1:T(8,128)(2,1)}) %all-gather.9.cloned.1.call-update) | async-done | bytes 4194320 | tf_op jit(solution)/shard_map/all_gather | solution.py:107
  87.4 3.0 %convolution_convert_fusion.1 = bf16[1024,16]{0,1:T(8,128)(2,1)S(1)} fusion(bf16[1024,2048]{0,1:T(8,128)(2,1)} %all-gather.9.cloned.1.call-done, bf16[2,2048,16]{1,2,0:T(8,128)(2,1)} %param.14), kind=kOutput, calls=%fused_computation.33 | convolution fusion | flops 67125248 | bytes 4292608 | tf_op jit(solution)/shard_map/dot_general | solution.py:110
  90.4 0.2 convolution_add_fusion.3
  90.6 0.1 fusion.64
  90.8 0.2 convolution_add_fusion.2
  91.0 0.2 fusion.40
  91.2 0.7 fusion.25
  91.9 27.8 %all-gather = bf16[16384,16]{0,1:T(8,128)(2,1)S(1)} all-gather(bf16[1024,16]{0,1:T(8,128)(2,1)S(1)} %fusion.25), channel_id=2, replica_groups=mesh['grp'=4,'tp_0'=16,'tp_1'=2] {'tp_0'}, dimensions={0}, use_global_device_ids=true | all-gather | bytes 557056 | tf_op jit(solution)/shard_map/all_gather | solution.py:34
  119.7 0.8 copy.58
  120.6 0.1 all-gather.15.cloned.1.call-start
  120.7 6.6 %copy.39 = bf16[1024,2048]{1,0:T(8,128)(2,1)} copy(bf16[1024,2048]{0,1:T(8,128)(2,1)} %all-gather.9.cloned.1.call-done) | data formatting | bytes 8388608 | tf_op jit(solution)/shard_map/all_gather | solution.py:107
  127.2 30.5 %all-gather.11.cloned.1.call-done = bf16[2048,1028]{1,0:T(8,128)(2,1)} async-done(((bf16[64,1028]{1,0:T(8,128)(2,1)}), bf16[2048,1028]{1,0:T(8,128)(2,1)}) %all-gather.11.cloned.1.call-update) | async-done | bytes 4210704 | tf_op jit(solution)/shard_map/all_gather | solution.py:17
  157.7 1.1 slice.178
  158.8 0.2 copy.45
  159.0 4.7 %slice.176 = bf16[2048,1024]{1,0:T(8,128)(2,1)} slice(bf16[2048,1028]{1,0:T(8,128)(2,1)} %all-gather.11.cloned.1.call-done), slice={[0:2048], [0:1024]} | slice | bytes 8388608 | tf_op jit(solution)/shard_map/slice | solution.py:19
  163.7 6.6 %copy.51 = bf16[2048,1024]{0,1:T(8,128)(2,1)} copy(bf16[2048,1024]{1,0:T(8,128)(2,1)} %slice.176) | data formatting | bytes 8388608 | tf_op jit(solution)/shard_map/reshape | solution.py:19
  170.3 3.0 %all-gather.13.cloned.1.call-done = bf16[32,1024,16]{1,2,0:T(8,128)(2,1)} async-done(((bf16[16,1024,16]{1,2,0:T(8,128)(2,1)}), bf16[32,1024,16]{1,2,0:T(8,128)(2,1)}) %all-gather.13.cloned.1.call-update) | async-done | bytes 1048592 | tf_op jit(solution)/shard_map/all_gather | solution.py:34
  173.3 1.3 copy.41
  174.6 6.0 %convert_reduce_fusion = (f32[1024]{0:T(1024)S(1)}, f32[1024]{0:T(1024)S(1)}, bf16[1024,2048]{1,0:T(8,128)(2,1)S(1)}) fusion(bf16[1024,512]{0,1:T(8,128)(2,1)S(1)} %bitcast.323, bf16[2,512,2048]{2,1,0:T(8,128)(2,1)} %bitcast.310, bf16[1024,2048]{1,0:T(8,128)(2,1)} %copy.39), kind=kOutput, calls=%fused_computation.2 | convolution fusion | flops 2164258816 | bytes 11542528 | tf_op jit(solution)/shard_map/dot_general | solution.py:128
  180.6 1.9 fusion.3
  182.5 1.2 convolution_convert_fusion.3
  183.7 0.2 convolution_add_fusion
  183.9 0.2 convolution_add_fusion.1
  184.2 0.1 fusion.57
  184.3 0.2 fusion.47
  184.4 1.2 fusion.24
  185.7 25.7 %all-gather.2 = bf16[16384,16]{0,1:T(8,128)(2,1)S(1)} all-gather(bf16[1024,16]{0,1:T(8,128)(2,1)S(1)} %fusion.24), channel_id=4, replica_groups=mesh['grp'=4,'tp_0'=16,'tp_1'=2] {'tp_0'}, dimensions={0}, use_global_device_ids=true | all-gather | bytes 557056 | tf_op jit(solution)/shard_map/all_gather | solution.py:34
  211.4 0.8 copy.57
  212.4 0.1 dynamic-slice
  212.4 0.1 dynamic-slice.1
  212.5 1.1 maximum_bitcast_fusion
  213.6 20.3 %all-gather.15.cloned.1.call-done = bf16[32,1024,16]{1,2,0:T(8,128)(2,1)} async-done(((bf16[16,1024,16]{1,2,0:T(8,128)(2,1)}), bf16[32,1024,16]{1,2,0:T(8,128)(2,1)}) %all-gather.15.cloned.1.call-update) | async-done | bytes 1048592 | tf_op jit(solution)/shard_map/all_gather | solution.py:34
  233.9 1.3 copy.47
  235.2 6.1 %fusion.102 = (f32[1024]{0:T(1024)S(1)}, f32[1024]{0:T(1024)S(1)}, f32[1024,2048]{1,0:T(8,128)S(1)}) fusion(bf16[1024,512]{0,1:T(8,128)(2,1)S(1)} %bitcast.322, bf16[2,512,2048]{2,1,0:T(8,128)(2,1)} %bitcast.311, bf16[1024,2048]{1,0:T(8,128)(2,1)} %copy-done), kind=kOutput, calls=%fused_computation.171 | convolution fusion | flops 2164258816 | bytes 15736832 | tf_op jit(solution)/shard_map/dot_general | solution.py:128
  241.3 0.5 fusion.29
  241.8 0.8 copy.49
  (23 shorter events, 0.3 us)
Async XLA Ops:
  7.2 83.2 %copy-start.5 = (f32[2,2,1,64,16]{3,4,2,1,0:T(8,128)S(1)}, f32[2,2,1,64,16]{3,4,2,1,0:T(8,128)}, u32[]{:S(2)}) copy-start(f32[2,2,1,64,16]{3,4,2,1,0:T(8,128)} %param.21) | copy-start | bytes 49156
  7.2 83.2 %copy-start.2 = (f32[2,2,1,64,1024]{4,3,2,1,0:T(8,128)S(1)}, f32[2,2,1,64,1024]{4,3,2,1,0:T(8,128)}, u32[]{:S(2)}) copy-start(f32[2,2,1,64,1024]{4,3,2,1,0:T(8,128)} %param.13) | copy-start | bytes 3145732
  7.2 83.4 %copy-start.6 = (f32[2,2,1,16,64]{4,3,2,1,0:T(8,128)S(1)}, f32[2,2,1,16,64]{4,3,2,1,0:T(8,128)}, u32[]{:S(2)}) copy-start(f32[2,2,1,16,64]{4,3,2,1,0:T(8,128)} %param.22) | copy-start | bytes 49156
  7.2 84.0 %copy-start.3 = (bf16[2,2048,16]{1,2,0:T(8,128)(2,1)S(1)}, bf16[2,2048,16]{1,2,0:T(8,128)(2,1)}, u32[]{:S(2)}) copy-start(bf16[2,2048,16]{1,2,0:T(8,128)(2,1)} %param.15) | copy-start | bytes 393220
  7.2 80.2 %all-gather.9.cloned.1.call-start = ((), (), s32[]{:S(2)}) async-start(), calls=%async_computation | async-start | bytes 4325376 | tf_op jit(solution)/shard_map/all_gather | solution.py:107
  8.0 149.7 %all-gather.11.cloned.1.call-start = ((), (), s32[]{:S(2)}) async-start(), calls=%async_computation.1 | async-start | bytes 4866048 | tf_op jit(solution)/shard_map/all_gather | solution.py:17
  10.5 162.8 %all-gather.13.cloned.1.call-start = ((), (), s32[]{:S(2)}) async-start(), calls=%async_computation.2 | async-start | bytes 1572864 | tf_op jit(solution)/shard_map/all_gather | solution.py:34
  87.4 3.8 %copy-start.1 = (bf16[1024,2048]{0,1:T(8,128)(2,1)S(1)}, bf16[1024,2048]{0,1:T(8,128)(2,1)}, u32[]{:S(2)}) copy-start(bf16[1024,2048]{0,1:T(8,128)(2,1)} %all-gather.9.cloned.1.call-done) | copy-start | bytes 12582916
  120.6 113.3 %all-gather.15.cloned.1.call-start = ((), (), s32[]{:S(2)}) async-start(), calls=%async_computation.3 | async-start | bytes 1572864 | tf_op jit(solution)/shard_map/all_gather | solution.py:34
  180.6 1.9 copy-start.4
  182.5 3.2 %copy-start = (bf16[1024,2048]{1,0:T(8,128)(2,1)}, bf16[1024,2048]{1,0:T(8,128)(2,1)S(1)}, u32[]{:S(2)}) copy-start(bf16[1024,2048]{1,0:T(8,128)(2,1)S(1)} %fusion.3) | copy-start | bytes 12582916
Sparse Core Ops, SparseCore 0:
  9.8 77.5 all-gather.8
  89.1 68.5 all-gather.10
  160.0 13.2 all-gather.12
  212.4 21.4 all-gather.14
where the time goes:
time: 250 us; the launch traced here: 249 us
  waiting for transfers between devices  126 us (50%)
  blocking collectives  53.5 us (21%)
  local copies, waits for them, and re-layouts  28.1 us (11%)
  matrix products  19.6 us (8%)
  between operations  15.4 us (6%)
  other arithmetic  6.37 us (3%)
    all_gather x1, waiting for transfers between devices, per_device(): whole_rows = lax.all_gather(tokens, TP, axis=1, tiled=True)  71.2 us
    all_gather x2, blocking collectives, all_blocks(): tiles = lax.all_gather(tiles, axes[k])  53.5 us
    all_gather x1, waiting for transfers between devices, gather_turned(): out, at, finished = (lax.all_gather(both, axis, axis=0, tiled=True), 0, [])  30.5 us
    all_gather x2, waiting for transfers between devices, all_blocks(): tiles = lax.all_gather(tiles, axes[k])  23.2 us
    dot_general x2, matrix products, per_device(): jnp.dot(gated_all, out_whole[layer_idx], preferred_element_type=jnp.float32)  12.1 us
    reshape x2, local copies, waits for them, and re-layouts, gather_turned(): piece = out[:, at:at + t[0].size].reshape(-1, *t.shape[1:])  6.58 us
    all_gather x1, local copies, waits for them, and re-layouts, per_device(): whole_rows = lax.all_gather(tokens, TP, axis=1, tiled=True)  6.56 us
    slice x3, local copies, waits for them, and re-layouts, gather_turned(): piece = out[:, at:at + t[0].size].reshape(-1, *t.shape[1:])  5.98 us
  transfers between devices with their start and end apart: 4, of which 4 were waited for; matrix products, arithmetic and copies ran while one was open for 13% of the time, Pallas kernels for 0%

commit v1 on v0

v1 whole, which is shorter than its diff:
```python
import functools

import jax
import jax.numpy as jnp
from jax import lax
from jax.experimental import pallas as pl
from jax.experimental.pallas import tpu as pltpu
from jax.sharding import PartitionSpec as P

MESH = pl.DeviceIdType.MESH
bf16, f32 = jnp.bfloat16, jnp.float32

residual_scale = 1.4142135623730951
norm_eps = 1e-05


def tile(start, size):
    return pl.ds(pl.multiple_of(start, size), size)


class Ring:
    def __init__(self, nz, own, buf, per, pieces, send, recv, give, take):
        self.nz, self.own, self.buf, self.per, self.pieces = nz, own, buf, per, pieces
        self.send_sem, self.recv_sem, self.give_sem, self.take_sem = send, recv, give, take
        me = lax.axis_index("tp")
        self.z, self.c = me // 2, lax.rem(me, 2)
        self.me, self.sib = me, self.z * 2 + (1 - self.c)
        self.next = (lax.rem(self.z + 1, nz) * 2 + self.c, lax.rem(self.z + nz - 1, nz) * 2 + self.c)
        self.half = nz // 2

    def origin(self, way, s, core):
        z = lax.rem(self.z - s + self.nz, self.nz) if way == 0 else lax.rem(self.z + s, self.nz)
        return z * 2 + core

    def parts(self, way, s):
        if s < self.half:
            n = self.pieces
            return [(i * self.per // n, self.per // n) for i in range(n)]
        return [(way * self.per // 2, self.per // 2)]

    def place(self, dev, part):
        start, size = part
        return self.buf.at[pl.ds(pl.multiple_of(dev * self.per + start, size), size)]

    def hop(self, way, s, i):
        part = self.parts(way, s)[i]
        src_dev = self.origin(way, s - 1, self.c)
        src = self.own.at[pl.ds(*part)] if s == 1 and self.own is not None else self.place(src_dev, part)
        return pltpu.make_async_remote_copy(
            src_ref=src,
            dst_ref=self.place(src_dev, part),
            send_sem=self.send_sem.at[way, s - 1, i],
            recv_sem=self.recv_sem.at[way, s - 1, i],
            device_id={"tp": self.next[way]},
            device_id_type=MESH,
        )

    def start(self, way, s, i):
        self.hop(way, s, i).start()

    def arrive(self, way, s, i):
        part = self.parts(way, s)[i]
        dst = self.place(self.origin(way, s, self.c), part)
        pltpu.make_async_remote_copy(
            src_ref=dst,
            dst_ref=dst,
            send_sem=self.send_sem.at[way, s - 1, i],
            recv_sem=self.recv_sem.at[way, s - 1, i],
            device_id={"tp": self.next[way]},
            device_id_type=MESH,
        ).wait_recv()

    def whole(self, way, s):
        return (0, self.per) if s < self.half else self.parts(way, s)[0]

    def handover(self, way, s, core):
        part = self.whole(way, s)
        dev = self.origin(way, s, core)
        src = self.own if s == 0 and self.own is not None else self.place(dev, part)
        return pltpu.make_async_remote_copy(
            src_ref=src,
            dst_ref=self.place(dev, part),
            send_sem=self.give_sem.at[way, s],
            recv_sem=self.take_sem.at[way, s],
            device_id={"tp": self.sib},
            device_id_type=MESH,
        )

    def begin(self):
        for i in range(self.pieces):
            for way in range(2):
                if self.half > 1:
                    self.start(way, 1, i)
        if self.half == 1:
            for way in range(2):
                self.start(way, 1, 0)
        self.handover(0, 0, self.c).start()

    def step(self, s):
        n = max(len(self.parts(0, s)), 1)
        for i in range(n):
            for way in range(2):
                self.arrive(way, s, i)
                if s + 1 < self.half:
                    self.start(way, s + 1, i)
        if s + 1 == self.half:
            for way in range(2):
                self.start(way, s + 1, 0)
        for way in range(2):
            self.handover(way, s, self.c).start()

    def other(self, s):
        for way in range(2 if s else 1):
            dev = self.origin(way, s, 1 - self.c)
            dst = self.place(dev, self.whole(way, s))
            pltpu.make_async_remote_copy(
                src_ref=dst,
                dst_ref=dst,
                send_sem=self.give_sem.at[way, s],
                recv_sem=self.take_sem.at[way, s],
                device_id={"tp": self.sib},
                device_id_type=MESH,
            ).wait_recv()

    def finish(self):
        for s in range(1, self.half + 1):
            for way in range(2):
                for i in range(len(self.parts(way, s))):
                    self.hop(way, s, i).wait_send()
        for s in range(self.half + 1):
            for way in range(2 if s else 1):
                self.handover(way, s, self.c).wait_send()


def dot(a, b):
    return jnp.dot(a, b, preferred_element_type=f32)


def kernel(
    nz,
    tok,
    carried,
    win,
    wgate,
    wout,
    norm,
    lam_re,
    lam_im,
    log_step,
    in_c,
    out_c,
    skip,
    out,
    new_carried,
    x_all,
    s_all,
    w_all,
    g_all,
    p_own,
    p_all,
    gain_b,
    bias_b,
    w_in,
    push_w,
    push_t,
    read_w,
    cols,
    cols_t,
    held,
    fresh,
    acc,
    x_sem,
    xd_sem,
    w_sem,
    wd_sem,
    g_sem,
    gd_sem,
    p_sem,
    pd_sem,
    io_sem,
):
    layers, half = 2, nz // 2
    ndev = 2 * nz
    width, batch = x_all.shape
    per = tok.shape[0]
    ch = win.shape[1]
    state = held.shape[2]
    me = lax.axis_index("tp")

    xr = Ring(nz, tok, x_all, per, 2, x_sem.at[0], x_sem.at[1], xd_sem.at[0], xd_sem.at[1])
    pr = Ring(nz, p_own, p_all, 16, 1, p_sem.at[0], p_sem.at[1], pd_sem.at[0], pd_sem.at[1])
    wr = [
        Ring(nz, wout.at[i], w_all.at[i], per, 1, w_sem.at[i, 0], w_sem.at[i, 1], wd_sem.at[i, 0], wd_sem.at[i, 1])
        for i in range(layers)
    ]
    gr = [
        Ring(nz, None, g_all.at[i], ch, 1, g_sem.at[i, 0], g_sem.at[i, 1], gd_sem.at[i, 0], gd_sem.at[i, 1])
        for i in range(layers)
    ]

    barrier = pltpu.get_barrier_semaphore()
    for dev in (*xr.next, xr.sib):
        pl.semaphore_signal(barrier, inc=1, device_id={"tp": dev}, device_id_type=MESH)
    load = pltpu.make_async_copy(carried, held, io_sem.at[0])
    load.start()
    p_own[...] = jnp.zeros_like(p_own)
    p_own[0:4, 0:per] = norm[...].astype(f32)
    pl.semaphore_wait(barrier, 3)

    xr.begin()
    pr.begin()

    x_all[tile(me * per, per)] = tok[...]
    p_all[tile(me * 16, 16)] = p_own[...]
    for l in range(layers):
        w_all[l, tile(me * per, per)] = wout[l]
        w_in[l, 0:ch] = win[l]
        w_in[l, ch : 2 * ch] = wgate[l]
    cols[...] = jnp.zeros_like(cols)
    for l in range(layers):
        re, im = lam_re[l], lam_im[l]
        step_len = jnp.exp(log_step[l : l + 1, 0:1])
        modulus = jnp.exp(re * step_len)
        decay_re = modulus * jnp.cos(im * step_len)
        decay_im = modulus * jnp.sin(im * step_len)
        denominator = re * re + im * im
        shifted = decay_re - 1.0
        coef_re = (shifted * re + decay_im * im) / denominator
        coef_im = (decay_im * re - shifted * im) / denominator
        in_re = coef_re * in_c[l, 0] - coef_im * in_c[l, 1]
        in_im = coef_re * in_c[l, 1] + coef_im * in_c[l, 0]
        push_t[l] = jnp.zeros_like(push_t[l])
        for k, v in enumerate((in_re, in_im)):
            high = v.astype(bf16).astype(f32)
            push_t[l, 0:ch, k * state : (k + 1) * state] = high
            push_t[l, ch : 2 * ch, k * state : (k + 1) * state] = v - high
        push_w[l] = push_t[l].T.astype(bf16)
        read_w[l, :, 0:state] = out_c[l, 0].astype(bf16)
        read_w[l, :, state : 2 * state] = (-out_c[l, 1]).astype(bf16)
        cols[8 * l : 8 * l + 1, 0:state] = decay_re
        cols[8 * l + 1 : 8 * l + 2, 0:state] = decay_im
        cols[8 * l + 2 : 8 * l + 3, 0:ch] = skip[l : l + 1]
    cols[3:5, 0:per] = norm[2:4].astype(f32)
    cols_t[...] = cols[...].T

    def gain_columns():
        for d in range(ndev):
            if d % 8 == 0:
                turned = p_all[d * 16 : (d + 8) * 16].T
            at = (d % 8) * 16
            gain_b[d * per : (d + 1) * per] = jnp.broadcast_to(turned[0:per, at : at + 1], (per, 128))
            bias_b[d * per : (d + 1) * per] = jnp.broadcast_to(turned[0:per, at + 1 : at + 2], (per, 128))

    def meet(dev_z):
        k = tile(dev_z * 2 * per, 2 * per)
        acc[...] += dot(w_in[0, :, k], x_all[k])

    acc[...] = jnp.zeros_like(acc)
    for s in range(1, half + 1):
        pr.step(s)
        xr.step(s)
        xr.other(s - 1)
        pr.other(s - 1)
        if s == 1:
            meet(xr.z)
        else:
            for way in range(2):
                meet(xr.origin(way, s - 1, 0) // 2)
    wr[0].begin()
    xr.other(half)
    pr.other(half)
    meet(xr.origin(0, half, 0) // 2)

    load.wait()

    def recur(l):
        span = min(256, batch)
        for j in range(batch // span):
            at = slice(j * span, (j + 1) * span)
            drive = acc[0:ch, at].astype(bf16)
            gate = acc[ch : 2 * ch, at].astype(bf16).astype(f32)
            pushed = dot(push_w[l, :, 0 : 2 * ch], jnp.concatenate([drive, drive], axis=0))
            decay_re = cols_t[0:state, 8 * l : 8 * l + 1]
            decay_im = cols_t[0:state, 8 * l + 1 : 8 * l + 2]
            old_re, old_im = held[l, 0, :, at], held[l, 1, :, at]
            re = decay_re * old_re - decay_im * old_im + pushed[0:state]
            im = decay_re * old_im + decay_im * old_re + pushed[state:]
            fresh[l, 0, :, at] = re
            fresh[l, 1, :, at] = im
            both = jnp.concatenate([re.astype(bf16), im.astype(bf16)], axis=0)
            y = dot(read_w[l], both) + cols_t[0:ch, 8 * l + 2 : 8 * l + 3] * drive.astype(f32)
            gated = jax.nn.gelu(y) * jax.nn.sigmoid(gate)
            g_all[l, tile(me * ch, ch), at] = gated.astype(bf16)
        return pltpu.make_async_copy(fresh.at[l], new_carried.at[l], io_sem.at[1 + l])

    def exchange(l):
        gr[l].begin()
        for s in range(1, half + 1):
            gr[l].step(s)
            wr[l].step(s)
            gr[l].other(s - 1)
            wr[l].other(s - 1)
        gr[l].other(half)
        wr[l].other(half)

    rows = 256
    spans = batch // 128

    def moments(l, src, keep):
        def body(t, sums):
            k = tile(t * rows, rows)
            mixed = dot(w_all[l, k], g_all[l])
            summed = (residual_scale * src[k].astype(f32) + mixed).astype(bf16)
            if keep is not None:
                keep[k] = summed
            wide = summed.astype(f32).reshape(rows // 8, 8, batch)
            return sums[0] + wide.sum(axis=0), sums[1] + (wide * wide).sum(axis=0)

        zero = jnp.zeros((8, batch), f32)
        total, squares = lax.fori_loop(0, width // rows, body, (zero, zero))
        mean = total.sum(axis=0, keepdims=True) / width
        var = squares.sum(axis=0, keepdims=True) / width - mean * mean
        return mean, lax.rsqrt(var + norm_eps)

    store = recur(0)
    store.start()
    exchange(0)
    gain_columns()
    mean, scale = moments(0, x_all, s_all)
    acc[...] = jnp.zeros_like(acc)

    def normed(t, _):
        k = tile(t * rows, rows)
        for j in range(spans):
            at = slice(j * 128, (j + 1) * 128)
            wide = (s_all[k, at].astype(f32) - mean[:, at]) * scale[:, at]
            s_all[k, at] = (wide * gain_b[k] + bias_b[k]).astype(bf16)
        acc[...] += dot(w_in[1, :, k], s_all[k])
        return 0

    lax.fori_loop(0, width // rows, normed, 0)
    wr[1].begin()
    store2 = recur(1)
    store2.start()
    exchange(1)
    mean, scale = moments(1, s_all, None)
    mine = tile(me * per, per)
    summed = (residual_scale * s_all[mine].astype(f32) + dot(wout[1], g_all[1])).astype(bf16).astype(f32)
    out[...] = ((summed - mean) * scale * cols_t[0:per, 3:4] + cols_t[0:per, 4:5]).astype(bf16)
    store.wait()
    store2.wait()
    for ring in (xr, pr, *wr, *gr):
        ring.finish()


def per_device(nz, tokens, carried, proj_in, proj_gate, proj_out, norm, lam_re, lam_im, log_step, in_c, out_c, skip):
    batch, per = tokens.shape
    layers, width, ch = proj_in.shape
    ssm = proj_out.shape[1]
    state = carried.shape[3]
    half = nz // 2
    vmem = pl.BlockSpec(memory_space=pltpu.VMEM)
    hbm = pl.BlockSpec(memory_space=pl.ANY)
    dma = pltpu.SemaphoreType.DMA
    out, fresh = pl.pallas_call(
        functools.partial(kernel, nz),
        out_shape=(
            jax.ShapeDtypeStruct((per, batch), bf16),
            jax.ShapeDtypeStruct((layers, 2, state, batch), f32),
        ),
        in_specs=[vmem, hbm] + [vmem] * 10,
        out_specs=(vmem, hbm),
        scratch_shapes=[
            pltpu.VMEM((width, batch), bf16),
            pltpu.VMEM((width, batch), bf16),
            pltpu.VMEM((layers, width, ssm), bf16),
            pltpu.VMEM((layers, ssm, batch), bf16),
            pltpu.VMEM((16, 128), f32),
            pltpu.VMEM((2 * nz * 16, 128), f32),
            pltpu.VMEM((width, 128), f32),
            pltpu.VMEM((width, 128), f32),
            pltpu.VMEM((layers, 2 * ch, width), bf16),
            pltpu.VMEM((layers, 128, 128), bf16),
            pltpu.VMEM((layers, 128, 128), f32),
            pltpu.VMEM((layers, ch, 2 * state), bf16),
            pltpu.VMEM((128, 128), f32),
            pltpu.VMEM((128, 128), f32),
            pltpu.VMEM((layers, 2, state, batch), f32),
            pltpu.VMEM((layers, 2, state, batch), f32),
            pltpu.VMEM((2 * ch, batch), f32),
            dma((2, 2, half, 2)),
            dma((2, 2, half + 1)),
            dma((layers, 2, 2, half, 1)),
            dma((layers, 2, 2, half + 1)),
            dma((layers, 2, 2, half, 1)),
            dma((layers, 2, 2, half + 1)),
            dma((2, 2, half, 1)),
            dma((2, 2, half + 1)),
            dma((3,)),
        ],
        compiler_params=pltpu.CompilerParams(
            collective_id=0, has_side_effects=True, vmem_limit_bytes=56 * 1024 * 1024
        ),
    )(
        tokens.T,
        carried.reshape(layers, 2, state, batch),
        proj_in.transpose(0, 2, 1),
        proj_gate.transpose(0, 2, 1),
        proj_out.transpose(0, 2, 1),
        norm.reshape(2 * layers, per),
        lam_re,
        lam_im,
        log_step,
        in_c.reshape(layers, 2, state, ch).transpose(0, 1, 3, 2),
        out_c.reshape(layers, 2, ch, state),
        skip,
    )
    return out.T, fresh.reshape(carried.shape)


def solution(mesh):
    return jax.shard_map(
        functools.partial(per_device, mesh.shape["tp"] // 2),
        mesh=mesh,
        in_specs=(
            P("grp", "tp"),
            P(None, None, "tp", None, "grp"),
            P(None, None, "tp"),
            P(None, None, "tp"),
            P(None, None, "tp"),
            P(None, None, "tp"),
            P(None, "tp", None),
            P(None, "tp", None),
            P(None, "tp"),
            P(None, None, "tp", None, None),
            P(None, None, "tp", None, None),
            P(None, "tp"),
        ),
        out_specs=(P("grp", "tp"), P(None, None, "tp", None, "grp")),
        check_vma=False,
    )
```

time: 250 us -> 136 us (0.54)
  Pallas kernels: 0 us -> 130 us
  waiting for transfers between devices: 126 us -> 0 us
  blocking collectives: 53.5 us -> 0 us
  local copies, waits for them, and re-layouts: 28.1 us -> 5.17 us
  matrix products: 19.6 us -> 0 us
  between operations: 15.4 us -> 0.65 us
  other arithmetic: 6.37 us -> 0 us
    pallas_call x0 -> x1, Pallas kernels: none -> 130 us  [per_device(): pl.pallas_call(functools.partial(kernel, nz), out_shape=(jax.ShapeDtypeSt...]
    all_gather x4 -> x0, waiting for transfers between devices: 125 us -> none  [the longest x1 71.2 us: per_device(): whole_rows = lax.all_gather(tokens, TP, axis=1, tiled=True)]
    all_gather x2 -> x0, blocking collectives: 53.5 us -> none  [all_blocks(): tiles = lax.all_gather(tiles, axes[k])]
    dot_general x14 -> x0, matrix products: 19.6 us -> none  [the longest x2 12.1 us: per_device(): jnp.dot(gated_all, out_whole[layer_idx], preferred_element_type=jnp.float32)]
    reshape x4 -> x0, local copies, waits for them, and re-layouts: 8.28 us -> none  [the longest x2 6.58 us: gather_turned(): piece = out[:, at:at + t[0].size].reshape(-1, *t.shape[1:])]
    all_gather x3 -> x0, local copies, waits for them, and re-layouts: 8.24 us -> none  [the longest x1 6.56 us: per_device(): whole_rows = lax.all_gather(tokens, TP, axis=1, tiled=True)]
    slice x4 -> x0, local copies, waits for them, and re-layouts: 7.29 us -> none  [the longest x3 5.98 us: gather_turned(): piece = out[:, at:at + t[0].size].reshape(-1, *t.shape[1:])]
    unnamed x15 -> x5, local copies, waits for them, and re-layouts: 0.82 us -> 5.17 us
  transfers between devices with their start and end apart: 4 -> 0, of which waited for: 4 -> 0; matrix products, arithmetic and copies ran while one was open for 13% -> 0% of each run, Pallas kernels for 0% -> 0%
where the time goes in v1:
time: 136 us
  Pallas kernels  130 us (96%)
  local copies, waits for them, and re-layouts  5.17 us (4%)
    pallas_call x1, Pallas kernels, per_device(): pl.pallas_call(functools.partial(kernel, nz), out_shape=(jax.ShapeDtypeSt...  130 us
    unnamed x5, local copies, waits for them, and re-layouts  5.17 us

profile of v1, /device:TPU:69, one launch (start us, length us, event | category | flops | bytes accessed | tf_op | source)
XLA Modules:
  0.0 135.6 jit_solution(15709029134740449431)
XLA Ops:
  0.6 0.0 copy-start
  0.6 0.6 copy-done
  1.3 0.6 copy.14.log_step
  1.9 129.8 %shard_map.131 = (bf16[64,1024]{1,0:T(8,128)(2,1)}, f32[2,2,64,1024]{3,2,1,0:T(8,128)}) custom-call(bf16[64,1024]{1,0:T(8,128)(2,1)} %bitcast.17, f32[2,2,64,1024]{3,2,1,0:T(8,128)} %bitcast.14, bf16[2,16,2048]{2,1,0:T(8,128)(2,1)} %bitcast.18, bf16[2,16,2048]{2,1,0:T(8,128)(2,1)} %bitcast.19, bf16[2,64,512]{2,1,0:T(8,128)(2,1)} %bitcast.20, ...), custom_call_target="tpu_custom_call" | custom-call | tf_op jit(solution)/shard_map/pallas_call | solution.py:365
  131.8 1.6 %copy.18 = bf16[1024,64]{0,1:T(8,128)(2,1)} copy(bf16[1024,64]{0,1:T(8,128)(2,1)} %bitcast.16) | data formatting | bytes 262144
  133.3 2.3 %copy.19 = f32[2,2,1,64,1024]{4,3,2,1,0:T(8,128)} copy(f32[2,2,1,64,1024]{4,3,2,1,0:T(8,128)} %bitcast.15) | data formatting | bytes 2097152
Async XLA Ops:
  0.6 0.7 copy-start

commit v2 on v1

v2 whole, which is shorter than its diff:
```python
import functools

import jax
import jax.numpy as jnp
from jax import lax
from jax.experimental import pallas as pl
from jax.experimental.pallas import tpu as pltpu
from jax.sharding import PartitionSpec as P

MESH = pl.DeviceIdType.MESH
bf16, f32 = jnp.bfloat16, jnp.float32

residual_scale = 1.4142135623730951
norm_eps = 1e-05

X_PIECES = 2
W_PIECES = 2
STRIDE = 2
W_LEAD = 6
VMEM_MIB = 56
W_RELAY = (1, 0)
P_RELAY = 1


def tile(start, size):
    return pl.ds(pl.multiple_of(start, size), size)


class Place:
    def __init__(self, nz):
        me = lax.axis_index("tp")
        self.nz, self.half = nz, nz // 2
        self.me, self.z, self.c = me, me // 2, lax.rem(me, 2)
        self.sib = self.z * 2 + (1 - self.c)

    def away(self, way, s):
        return lax.rem(self.z + (s if way == 0 else self.nz - s), self.nz)

    def origin(self, way, s):
        return self.away(1 - way, s)

    def carries(self, way, s, core):
        return s < self.half or (s == self.half and (way == 0) == (core == 1))


class Gather:
    def __init__(self, at, relay, own, buf, per, pieces, stride, send, recv, give, take):
        self.relay, self.relays = relay, at.c == relay
        self.at, self.own, self.buf, self.per, self.pieces, self.stride = at, own, buf, per, pieces, stride
        self.send_sem, self.recv_sem, self.give_sem, self.take_sem = send, recv, give, take

    def rows(self, start, size):
        return self.buf.at[pl.ds(pl.multiple_of(start, size), size)]

    def copy(self, way, s, core, i, by=1):
        at, size = self.at, self.per // self.pieces
        chip = at.origin(way, s - by)
        dst = self.rows((chip * 2 + core) * self.per + i * size, size)
        src = dst if s > by or self.own is None else self.own.at[pl.ds(i * size, size)]
        return pltpu.make_async_remote_copy(
            src_ref=src,
            dst_ref=dst,
            send_sem=self.send_sem,
            recv_sem=self.recv_sem.at[way, s - 1, core, i],
            device_id={"tp": at.away(way, by) * 2 + self.relay},
            device_id_type=MESH,
        )

    def arrive(self, way, s, core, i):
        size = self.per // self.pieces
        dst = self.rows((self.at.origin(way, s) * 2 + core) * self.per + i * size, size)
        pltpu.make_async_remote_copy(
            src_ref=dst,
            dst_ref=dst,
            send_sem=self.send_sem,
            recv_sem=self.recv_sem.at[way, s - 1, core, i],
            device_id={"tp": self.at.sib},
            device_id_type=MESH,
        ).wait_recv()

    def reach(self, s):
        if s % self.stride:
            return []
        return [s + by for by in range(self.stride, 0, -1) if s + by <= self.at.half]

    def span(self, way, s):
        chip = self.at.origin(way, s) * 2 * self.per
        if s < self.at.half:
            return self.rows(chip, 2 * self.per)
        return self.rows(chip + (self.per if way == 0 else 0), self.per)

    def handover(self, way, s):
        dst = self.span(way, s)
        return pltpu.make_async_remote_copy(
            src_ref=dst,
            dst_ref=dst,
            send_sem=self.give_sem,
            recv_sem=self.take_sem.at[s],
            device_id={"tp": self.at.sib},
            device_id_type=MESH,
        )

    def own_over(self):
        dst = self.rows(self.at.me * self.per, self.per)
        return pltpu.make_async_remote_copy(
            src_ref=dst if self.own is None else self.own,
            dst_ref=dst,
            send_sem=self.give_sem,
            recv_sem=self.take_sem.at[0],
            device_id={"tp": self.at.sib},
            device_id_type=MESH,
        )

    def sends(self, s, way, core):
        return [t for t in self.reach(s) if self.at.carries(way, t, core)]

    def begin(self):
        for core in range(2):

            @pl.when(self.at.c == core)
            def _():
                for t in self.reach(0):
                    for i in range(self.pieces):
                        for way in range(2):
                            if self.at.carries(way, t, core):
                                self.copy(way, t, core, i, t).start()

        self.own_over().start()

    def order(self):
        half, stride = self.at.half, self.stride
        out = []
        for k in range(0, half, stride):
            top = min(k + stride, half)
            out.append([top] + list(range(k + 1, top)))
        return out

    def step(self, s):
        @pl.when(self.relays)
        def _():
            for core in (self.relay, 1 - self.relay):
                for i in range(self.pieces):
                    for way in range(2):
                        if self.at.carries(way, s, core):
                            self.arrive(way, s, core, i)
                            for t in self.sends(s, way, core):
                                self.copy(way, t, core, i, t - s).start()
            for way in range(2):
                self.handover(way, s).start()

    def bulk(self, blocks, send=None, recv=None):
        ref = self.buf.at[pl.ds(0, blocks * self.per)]
        return pltpu.make_async_remote_copy(
            src_ref=ref,
            dst_ref=ref,
            send_sem=self.send_sem if send is None else send,
            recv_sem=self.take_sem.at[0] if recv is None else recv,
            device_id={"tp": self.at.sib},
            device_id_type=MESH,
        )

    def ready(self, s):
        if s == 0:
            self.bulk(1, recv=self.take_sem.at[0]).wait_recv()
            return

        @pl.when(jnp.logical_not(self.relays))
        def _():
            self.bulk(4 if s < self.at.half else 2, recv=self.take_sem.at[s]).wait_recv()

    def finish(self):
        half, every = self.at.half, [(way, core) for way in range(2) for core in range(2)]
        for core in range(2):
            sent = sum(self.at.carries(way, t, core) for t in self.reach(0) for way in range(2))
            given = 1
            if core == self.relay:
                sent += sum(len(self.sends(s, *who)) for s in range(1, half + 1) for who in every)
                given += 4 * (half - 1) + 2

            @pl.when(self.at.c == core)
            def _():
                self.bulk(sent).wait_send()
                self.bulk(given, send=self.give_sem).wait_send()


def dot(a, b):
    return jnp.dot(a, b, preferred_element_type=f32)


def kernel(
    nz,
    tok_in,
    carried,
    win,
    wgate,
    wout_in,
    norm_in,
    lam_re_in,
    lam_im_in,
    log_step_in,
    in_c_in,
    out_c_in,
    skip_in,
    out_to,
    new_carried,
    tok,
    wout,
    norm,
    lam_re,
    lam_im,
    log_step,
    in_c,
    out_c,
    skip,
    out,
    x_all,
    s_all,
    w_all,
    g_all,
    p_own,
    p_all,
    gain_b,
    bias_b,
    w_in,
    push_w,
    push_t,
    read_w,
    cols,
    cols_t,
    held,
    fresh,
    acc,
    x_sem,
    xd_sem,
    w_sem,
    wd_sem,
    g_sem,
    gd_sem,
    p_sem,
    pd_sem,
    in_sem,
    io_sem,
    sent,
):
    layers, half = 2, nz // 2
    ndev = 2 * nz
    width, batch = x_all.shape
    per = tok.shape[0]
    ch = win.shape[1]
    state = held.shape[2]
    place = Place(nz)
    me = place.me

    def gather(relay, own, buf, rows, pieces, stride, sem, over, out):
        return Gather(place, relay, own, buf, rows, pieces, stride, sent.at[2 * out], sem, sent.at[2 * out + 1], over)

    xr = gather(1, tok, x_all, per, X_PIECES, 1, x_sem, xd_sem, 0)
    pr = gather(P_RELAY, p_own, p_all, 8, 1, 1, p_sem, pd_sem, 1)
    wr = [gather(W_RELAY[i], wout.at[i], w_all.at[i], per, W_PIECES, 1, w_sem.at[i], wd_sem.at[i], 2 + i) for i in range(layers)]
    gr = [gather(1, None, g_all.at[i], ch, 1, STRIDE, g_sem.at[i], gd_sem.at[i], 4 + i) for i in range(layers)]

    barrier = pltpu.get_barrier_semaphore()
    reach = {core: max((r.stride for r in (xr, pr, *wr, *gr) if r.relay == core), default=0) for core in range(2)}

    def near(core):
        return [(way, s) for way in range(2) for s in range(1, min(reach[core], half) + 1) if way == 0 or 2 * s < nz]

    def here(dev):
        pl.semaphore_signal(barrier, inc=1, device_id={"tp": dev}, device_id_type=MESH)

    for core in range(2):

        @pl.when(place.c == core)
        def _():
            for way, s in near(core):
                for other in range(2):
                    here(place.away(way, s) * 2 + other)

    here(place.sib)
    sources = (tok_in, norm_in, wout_in, lam_re_in, lam_im_in, log_step_in, in_c_in, out_c_in, skip_in, carried)
    targets = (tok, norm, wout, lam_re, lam_im, log_step, in_c, out_c, skip, held)
    loads = [pltpu.make_async_copy(a, b, in_sem.at[i]) for i, (a, b) in enumerate(zip(sources, targets))]
    for k, w in enumerate((win, wgate)):
        for l in range(layers):
            part = w_in.at[l, pl.ds(k * ch, ch)]
            loads.append(pltpu.make_async_copy(w.at[l], part, in_sem.at[len(sources) + 2 * k + l]))
    for load in loads:
        load.start()
    loads[0].wait()
    loads[1].wait()
    p_own[...] = jnp.zeros_like(p_own)
    p_own[0:4, 0:per] = norm[...].astype(f32)
    pl.semaphore_wait(barrier, len(near(0)) + len(near(1)) + 1)

    xr.begin()
    pr.begin()
    for i, load in enumerate(loads):
        if i > 1 and i != len(sources) - 1:
            load.wait()

    x_all[tile(me * per, per)] = tok[...]
    p_all[tile(me * 8, 8)] = p_own[...]
    for l in range(layers):
        w_all[l, tile(me * per, per)] = wout[l]
    cols[...] = jnp.zeros_like(cols)
    for l in range(layers):
        re, im = lam_re[l], lam_im[l]
        step_len = jnp.exp(log_step[0:1, l : l + 1])
        modulus = jnp.exp(re * step_len)
        decay_re = modulus * jnp.cos(im * step_len)
        decay_im = modulus * jnp.sin(im * step_len)
        denominator = re * re + im * im
        shifted = decay_re - 1.0
        coef_re = (shifted * re + decay_im * im) / denominator
        coef_im = (decay_im * re - shifted * im) / denominator
        in_re = coef_re * in_c[l, 0] - coef_im * in_c[l, 1]
        in_im = coef_re * in_c[l, 1] + coef_im * in_c[l, 0]
        push_t[l] = jnp.zeros_like(push_t[l])
        for k, v in enumerate((in_re, in_im)):
            high = v.astype(bf16).astype(f32)
            push_t[l, 0:ch, k * state : (k + 1) * state] = high
            push_t[l, ch : 2 * ch, k * state : (k + 1) * state] = v - high
        push_w[l] = push_t[l].T.astype(bf16)
        read_w[l, :, 0:state] = out_c[l, 0].astype(bf16)
        read_w[l, :, state : 2 * state] = (-out_c[l, 1]).astype(bf16)
        cols[8 * l : 8 * l + 1, 0:state] = decay_re
        cols[8 * l + 1 : 8 * l + 2, 0:state] = decay_im
        cols[8 * l + 2 : 8 * l + 3, 0:ch] = skip[l : l + 1]
    cols[3:5, 0:per] = norm[2:4].astype(f32)
    cols_t[...] = cols[...].T

    def gain_columns():
        for d in range(ndev):
            if d % 16 == 0:
                turned = p_all[d * 8 : d * 8 + min(128, ndev * 8)].T
            at = (d % 16) * 8
            gain_b[d * per : (d + 1) * per] = jnp.broadcast_to(turned[0:per, at : at + 1], (per, 128))
            bias_b[d * per : (d + 1) * per] = jnp.broadcast_to(turned[0:per, at + 1 : at + 2], (per, 128))

    def meet(dev_z):
        k = tile(dev_z * 2 * per, 2 * per)
        acc[...] += dot(w_in[0, :, k], x_all[k])

    acc[...] = jnp.zeros_like(acc)
    w_first = max(half + 1 - W_LEAD, 0)
    if w_first == 0:
        wr[0].begin()
    for s in range(1, half + 1):
        xr.step(s)
        if s == w_first:
            wr[0].begin()
        if s > w_first:
            wr[0].step(s - w_first)
        pr.step(s)
        xr.ready(s - 1)
        if s == 1:
            meet(place.z)
        else:
            for way in range(2):
                meet(place.origin(way, s - 1))
    if W_LEAD == 0:
        wr[0].begin()
    xr.ready(half)
    meet(place.origin(0, half))
    w_next = max(min(W_LEAD, half), 1) if w_first else half + 1

    loads[len(sources) - 1].wait()

    def recur(l):
        span = min(256, batch)
        for j in range(batch // span):
            at = slice(j * span, (j + 1) * span)
            drive = acc[0:ch, at].astype(bf16)
            gate = acc[ch : 2 * ch, at].astype(bf16).astype(f32)
            pushed = dot(push_w[l, :, 0 : 2 * ch], jnp.concatenate([drive, drive], axis=0))
            decay_re = cols_t[0:state, 8 * l : 8 * l + 1]
            decay_im = cols_t[0:state, 8 * l + 1 : 8 * l + 2]
            old_re, old_im = held[l, 0, :, at], held[l, 1, :, at]
            re = decay_re * old_re - decay_im * old_im + pushed[0:state]
            im = decay_re * old_im + decay_im * old_re + pushed[state:]
            fresh[l, 0, :, at] = re
            fresh[l, 1, :, at] = im
            both = jnp.concatenate([re.astype(bf16), im.astype(bf16)], axis=0)
            y = dot(read_w[l], both) + cols_t[0:ch, 8 * l + 2 : 8 * l + 3] * drive.astype(f32)
            gated = jax.nn.gelu(y) * jax.nn.sigmoid(gate)
            g_all[l, tile(me * ch, ch), at] = gated.astype(bf16)
        return pltpu.make_async_copy(fresh.at[l], new_carried.at[l], io_sem.at[l])

    w_two = iter(range(half + 1))

    def further():
        s = next(w_two, None)
        if s == 0:
            wr[1].begin()
        elif s is not None:
            wr[1].step(s)

    def exchange(l, left):
        gr[l].begin()
        order = gr[l].order()
        if l == 0:
            further()
            for s in range(half + 1):
                pr.ready(s)
            gain_columns()
        for n, steps in enumerate(order):
            for s in steps:
                gr[l].step(s)
            upto = -(-len(left) // (len(order) - n))
            for s in left[:upto]:
                wr[l].step(s)
            left = left[upto:]
            if l == 0:
                further()
        for s in range(half + 1):
            gr[l].ready(s)
            wr[l].ready(s)

    rows = 256
    spans = batch // 128

    def moments(l, src, keep):
        def body(t, sums):
            k = tile(t * rows, rows)
            mixed = dot(w_all[l, k], g_all[l])
            summed = (residual_scale * src[k].astype(f32) + mixed).astype(bf16)
            if keep is not None:
                keep[k] = summed
            wide = summed.astype(f32).reshape(rows // 8, 8, batch)
            return sums[0] + wide.sum(axis=0), sums[1] + (wide * wide).sum(axis=0)

        zero = jnp.zeros((8, batch), f32)
        sums, tiles = (zero, zero), width // rows
        total, squares = lax.fori_loop(0, tiles, body, sums)
        mean = total.sum(axis=0, keepdims=True) / width
        var = squares.sum(axis=0, keepdims=True) / width - mean * mean
        return mean, lax.rsqrt(var + norm_eps)

    store = recur(0)
    store.start()
    exchange(0, list(range(w_next, half + 1)))
    mean, scale = moments(0, x_all, s_all)
    acc[...] = jnp.zeros_like(acc)

    def normed(t, _):
        k = tile(t * rows, rows)
        for j in range(spans):
            at = slice(j * 128, (j + 1) * 128)
            wide = (s_all[k, at].astype(f32) - mean[:, at]) * scale[:, at]
            s_all[k, at] = (wide * gain_b[k] + bias_b[k]).astype(bf16)
        acc[...] += dot(w_in[1, :, k], s_all[k])
        return 0

    tiles = width // rows
    lax.fori_loop(0, tiles, normed, 0)
    further()
    store2 = recur(1)
    store2.start()
    exchange(1, list(w_two))
    mean, scale = moments(1, s_all, None)
    mine = tile(me * per, per)
    summed = (residual_scale * s_all[mine].astype(f32) + dot(wout[1], g_all[1])).astype(bf16).astype(f32)
    out[...] = ((summed - mean) * scale * cols_t[0:per, 3:4] + cols_t[0:per, 4:5]).astype(bf16)
    last = pltpu.make_async_copy(out, out_to, io_sem.at[2])
    last.start()
    store.wait()
    store2.wait()
    last.wait()
    for ring in (xr, pr, *wr, *gr):
        ring.finish()


def hand_out(out_in, fresh_in, out, fresh, out_held, fresh_held, sem):
    layers = fresh.shape[0]
    pairs = [(out_in, out_held, out)]
    pairs += [(fresh_in.at[l, k], fresh_held.at[l, k], fresh.at[l, k]) for l in range(layers) for k in range(2)]
    into = [pltpu.make_async_copy(a, b, sem.at[0, i]) for i, (a, b, _) in enumerate(pairs)]
    onto = [pltpu.make_async_copy(b, c, sem.at[1, i]) for i, (_, b, c) in enumerate(pairs)]
    for copy in into:
        copy.start()
    for first, then in zip(into, onto):
        first.wait()
        then.start()
    for copy in onto:
        copy.wait()


def per_device(nz, tokens, carried, proj_in, proj_gate, proj_out, norm, lam_re, lam_im, log_step, in_c, out_c, skip):
    batch, per = tokens.shape
    layers, width, ch = proj_in.shape
    ssm = proj_out.shape[1]
    state = carried.shape[3]
    half = nz // 2
    hbm = pl.BlockSpec(memory_space=pl.ANY)
    dma = pltpu.SemaphoreType.DMA
    out, fresh = pl.pallas_call(
        functools.partial(kernel, nz),
        out_shape=(
            jax.ShapeDtypeStruct((per, batch), bf16),
            jax.ShapeDtypeStruct((layers, 2, state, batch), f32),
        ),
        in_specs=[hbm] * 12,
        out_specs=(hbm, hbm),
        scratch_shapes=[
            pltpu.VMEM((per, batch), bf16),
            pltpu.VMEM((layers, per, ssm), bf16),
            pltpu.VMEM((2 * layers, per), bf16),
            pltpu.VMEM((layers, 1, state), f32),
            pltpu.VMEM((layers, 1, state), f32),
            pltpu.VMEM((1, layers), f32),
            pltpu.VMEM((layers, 2, ch, state), f32),
            pltpu.VMEM((layers, 2, ch, state), f32),
            pltpu.VMEM((layers, ch), f32),
            pltpu.VMEM((per, batch), bf16),
            pltpu.VMEM((width, batch), bf16),
            pltpu.VMEM((width, batch), bf16),
            pltpu.VMEM((layers, width, ssm), bf16),
            pltpu.VMEM((layers, ssm, batch), bf16),
            pltpu.VMEM((8, 128), f32),
            pltpu.VMEM((2 * nz * 8, 128), f32),
            pltpu.VMEM((width, 128), f32),
            pltpu.VMEM((width, 128), f32),
            pltpu.VMEM((layers, 2 * ch, width), bf16),
            pltpu.VMEM((layers, 128, 128), bf16),
            pltpu.VMEM((layers, 128, 128), f32),
            pltpu.VMEM((layers, ch, 2 * state), bf16),
            pltpu.VMEM((128, 128), f32),
            pltpu.VMEM((128, 128), f32),
            pltpu.VMEM((layers, 2, state, batch), f32),
            pltpu.VMEM((layers, 2, state, batch), f32),
            pltpu.VMEM((2 * ch, batch), f32),
            dma((2, half, 2, X_PIECES)),
            dma((half + 1,)),
            dma((layers, 2, half, 2, W_PIECES)),
            dma((layers, half + 1)),
            dma((layers, 2, half, 2, 1)),
            dma((layers, half + 1)),
            dma((2, half, 2, 1)),
            dma((half + 1,)),
            dma((14,)),
            dma((3,)),
            dma((12,)),
        ],
        compiler_params=pltpu.CompilerParams(
            collective_id=0, has_side_effects=True, vmem_limit_bytes=VMEM_MIB * 1024 * 1024
        ),
    )(
        tokens.T,
        carried.reshape(layers, 2, state, batch),
        proj_in.transpose(0, 2, 1),
        proj_gate.transpose(0, 2, 1),
        proj_out.transpose(0, 2, 1),
        norm.reshape(2 * layers, per),
        lam_re,
        lam_im,
        log_step.T,
        in_c.reshape(layers, 2, state, ch).transpose(0, 1, 3, 2),
        out_c.reshape(layers, 2, ch, state),
        skip,
    )
    out, fresh = pl.pallas_call(
        hand_out,
        out_shape=(
            jax.ShapeDtypeStruct((per, batch), bf16),
            jax.ShapeDtypeStruct((layers, 2, state, batch), f32),
        ),
        in_specs=[hbm, hbm],
        out_specs=(hbm, hbm),
        scratch_shapes=[
            pltpu.VMEM((per, batch), bf16),
            pltpu.VMEM((layers, 2, state, batch), f32),
            dma((2, 1 + 2 * layers)),
        ],
    )(out, fresh)
    return out.T, fresh.reshape(carried.shape)


def solution(mesh):
    return jax.shard_map(
        functools.partial(per_device, mesh.shape["tp"] // 2),
        mesh=mesh,
        in_specs=(
            P("grp", "tp"),
            P(None, None, "tp", None, "grp"),
            P(None, None, "tp"),
            P(None, None, "tp"),
            P(None, None, "tp"),
            P(None, None, "tp"),
            P(None, "tp", None),
            P(None, "tp", None),
            P(None, "tp"),
            P(None, None, "tp", None, None),
            P(None, None, "tp", None, None),
            P(None, "tp"),
        ),
        out_specs=(P("grp", "tp"), P(None, None, "tp", None, "grp")),
        check_vma=False,
    )
```

time: 136 us -> 99.1 us (0.73)
  Pallas kernels: 130 us -> 98.3 us
  local copies, waits for them, and re-layouts: 5.17 us -> 0 us
    pallas_call x1, Pallas kernels: 130 us -> 96.3 us  [per_device(): pl.pallas_call(functools.partial(kernel, nz), out_shape=(jax.ShapeDtypeSt...]
    unnamed x5 -> x0, local copies, waits for them, and re-layouts: 5.17 us -> none
    pallas_call x0 -> x1, Pallas kernels: none -> 2.07 us  [per_device(): pl.pallas_call(hand_out, out_shape=(jax.ShapeDtypeStruct((per, batch), bf...]
where the time goes in v2:
time: 99.1 us; the launch traced here: 99 us
  Pallas kernels  98.3 us (99%)
    pallas_call x1, Pallas kernels, per_device(): pl.pallas_call(functools.partial(kernel, nz), out_shape=(jax.ShapeDtypeSt...  96.3 us
    pallas_call x1, Pallas kernels, per_device(): pl.pallas_call(hand_out, out_shape=(jax.ShapeDtypeStruct((per, batch), bf...  2.07 us

profile of v2, /device:TPU:69, one launch (start us, length us, event | category | flops | bytes accessed | tf_op | source)
XLA Modules:
  0.0 99.0 jit_solution(3778956733147000621)
XLA Ops:
  0.6 96.3 %shard_map.131 = (bf16[64,1024]{1,0:T(8,128)(2,1)}, f32[2,2,64,1024]{3,2,1,0:T(8,128)}) custom-call(bf16[64,1024]{1,0:T(8,128)(2,1)} %bitcast.16, f32[2,2,64,1024]{3,2,1,0:T(8,128)} %bitcast.15, bf16[2,16,2048]{2,1,0:T(8,128)(2,1)} %bitcast.17, bf16[2,16,2048]{2,1,0:T(8,128)(2,1)} %bitcast.18, bf16[2,64,512]{2,1,0:T(8,128)(2,1)} %bitcast.19, ...), custom_call_target="tpu_custom_call" | custom-call | tf_op jit(solution)/shard_map/pallas_call | solution.py:496
  96.9 2.1 %shard_map.132 = (bf16[64,1024]{1,0:T(8,128)(2,1)}, f32[2,2,64,1024]{3,2,1,0:T(8,128)}) custom-call(bf16[64,1024]{1,0:T(8,128)(2,1)} %get-tuple-element.6.out_in, f32[2,2,64,1024]{3,2,1,0:T(8,128)} %get-tuple-element.7.fresh_in), custom_call_target="tpu_custom_call" | custom-call | tf_op jit(solution)/shard_map/pallas_call | solution.py:561

commit v3 on v2

--- a/solution.py
+++ b/solution.py
@@ -16,6 +16,10 @@
 X_PIECES = 2
 W_PIECES = 2
 STRIDE = 2
+EARLY = 1
+SPAN = 1024
+TALL = 2048
+GAIN_ROWS = 512
 W_LEAD = 6
 VMEM_MIB = 56
 W_RELAY = (1, 0)
@@ -366,24 +370,32 @@
 
     loads[len(sources) - 1].wait()
 
-    def recur(l):
-        span = min(256, batch)
-        for j in range(batch // span):
-            at = slice(j * span, (j + 1) * span)
-            drive = acc[0:ch, at].astype(bf16)
-            gate = acc[ch : 2 * ch, at].astype(bf16).astype(f32)
-            pushed = dot(push_w[l, :, 0 : 2 * ch], jnp.concatenate([drive, drive], axis=0))
-            decay_re = cols_t[0:state, 8 * l : 8 * l + 1]
-            decay_im = cols_t[0:state, 8 * l + 1 : 8 * l + 2]
-            old_re, old_im = held[l, 0, :, at], held[l, 1, :, at]
-            re = decay_re * old_re - decay_im * old_im + pushed[0:state]
-            im = decay_re * old_im + decay_im * old_re + pushed[state:]
-            fresh[l, 0, :, at] = re
-            fresh[l, 1, :, at] = im
-            both = jnp.concatenate([re.astype(bf16), im.astype(bf16)], axis=0)
-            y = dot(read_w[l], both) + cols_t[0:ch, 8 * l + 2 : 8 * l + 3] * drive.astype(f32)
-            gated = jax.nn.gelu(y) * jax.nn.sigmoid(gate)
-            g_all[l, tile(me * ch, ch), at] = gated.astype(bf16)
+    span = min(SPAN, batch)
+
+    def recur(l, at):
+        drive = acc[0:ch, at].astype(bf16)
+        gate = acc[ch : 2 * ch, at].astype(bf16).astype(f32)
+        pushed = dot(push_w[l, :, 0 : 2 * ch], jnp.concatenate([drive, drive], axis=0))
+        decay_re = cols_t[0:state, 8 * l : 8 * l + 1]
+        decay_im = cols_t[0:state, 8 * l + 1 : 8 * l + 2]
+        old_re, old_im = held[l, 0, :, at], held[l, 1, :, at]
+        re = decay_re * old_re - decay_im * old_im + pushed[0:state]
+        im = decay_re * old_im + decay_im * old_re + pushed[state:]
+        fresh[l, 0, :, at] = re
+        fresh[l, 1, :, at] = im
+        both = jnp.concatenate([re.astype(bf16), im.astype(bf16)], axis=0)
+        y = dot(read_w[l], both) + cols_t[0:ch, 8 * l + 2 : 8 * l + 3] * drive.astype(f32)
+        gated = jax.nn.gelu(y) * jax.nn.sigmoid(gate)
+        g_all[l, tile(me * ch, ch), at] = gated.astype(bf16)
+
+    def spans(work):
+        def body(j, _):
+            work(tile(j * span, span))
+            return 0
+
+        lax.fori_loop(0, batch // span, body, 0)
+
+    def store(l):
         return pltpu.make_async_copy(fresh.at[l], new_carried.at[l], io_sem.at[l])
 
     w_two = iter(range(half + 1))
@@ -416,55 +428,61 @@
             gr[l].ready(s)
             wr[l].ready(s)
 
-    rows = 256
-    spans = batch // 128
-
-    def moments(l, src, keep):
+    tall = min(TALL, width)
+
+    def moments(l, src, keep, at):
         def body(t, sums):
-            k = tile(t * rows, rows)
-            mixed = dot(w_all[l, k], g_all[l])
-            summed = (residual_scale * src[k].astype(f32) + mixed).astype(bf16)
+            k = tile(t * tall, tall)
+            mixed = dot(w_all[l, k], g_all[l, :, at])
+            summed = (residual_scale * src[k, at].astype(f32) + mixed).astype(bf16)
             if keep is not None:
-                keep[k] = summed
-            wide = summed.astype(f32).reshape(rows // 8, 8, batch)
+                keep[k, at] = summed
+            wide = summed.astype(f32).reshape(tall // 8, 8, span)
             return sums[0] + wide.sum(axis=0), sums[1] + (wide * wide).sum(axis=0)
 
-        zero = jnp.zeros((8, batch), f32)
-        sums, tiles = (zero, zero), width // rows
-        total, squares = lax.fori_loop(0, tiles, body, sums)
+        zero = jnp.zeros((8, span), f32)
+        total, squares = lax.fori_loop(0, width // tall, body, (zero, zero))
         mean = total.sum(axis=0, keepdims=True) / width
         var = squares.sum(axis=0, keepdims=True) / width - mean * mean
         return mean, lax.rsqrt(var + norm_eps)
 
-    store = recur(0)
-    store.start()
+    def first_norm(at):
+        mean, scale = moments(0, x_all, s_all, at)
+        gain_rows = min(GAIN_ROWS, width)
+
+        def normed(t, _):
+            k = tile(t * gain_rows, gain_rows)
+            wide = (s_all[k, at].astype(f32) - mean) * scale
+            gain, bias = gain_b[k], bias_b[k]
+            pieces = [wide[:, i : i + 128] * gain + bias for i in range(0, span, 128)]
+            s_all[k, at] = jnp.concatenate(pieces, axis=1).astype(bf16)
+            return 0
+
+        lax.fori_loop(0, width // gain_rows, normed, 0)
+        acc[:, at] = dot(w_in[1], s_all[:, at])
+        recur(1, at)
+
+    mine = tile(me * per, per)
+
+    def last_norm(at):
+        mean, scale = moments(1, s_all, None, at)
+        mixed = dot(wout[1], g_all[1, :, at])
+        summed = (residual_scale * s_all[mine, at].astype(f32) + mixed).astype(bf16).astype(f32)
+        out[:, at] = ((summed - mean) * scale * cols_t[0:per, 3:4] + cols_t[0:per, 4:5]).astype(bf16)
+
+    spans(functools.partial(recur, 0))
+    store(0).start()
     exchange(0, list(range(w_next, half + 1)))
-    mean, scale = moments(0, x_all, s_all)
-    acc[...] = jnp.zeros_like(acc)
-
-    def normed(t, _):
-        k = tile(t * rows, rows)
-        for j in range(spans):
-            at = slice(j * 128, (j + 1) * 128)
-            wide = (s_all[k, at].astype(f32) - mean[:, at]) * scale[:, at]
-            s_all[k, at] = (wide * gain_b[k] + bias_b[k]).astype(bf16)
-        acc[...] += dot(w_in[1, :, k], s_all[k])
-        return 0
-
-    tiles = width // rows
-    lax.fori_loop(0, tiles, normed, 0)
-    further()
-    store2 = recur(1)
-    store2.start()
+    spans(first_norm)
+    store(1).start()
+    if EARLY:
+        further()
     exchange(1, list(w_two))
-    mean, scale = moments(1, s_all, None)
-    mine = tile(me * per, per)
-    summed = (residual_scale * s_all[mine].astype(f32) + dot(wout[1], g_all[1])).astype(bf16).astype(f32)
-    out[...] = ((summed - mean) * scale * cols_t[0:per, 3:4] + cols_t[0:per, 4:5]).astype(bf16)
+    spans(last_norm)
     last = pltpu.make_async_copy(out, out_to, io_sem.at[2])
     last.start()
-    store.wait()
-    store2.wait()
+    store(0).wait()
+    store(1).wait()
     last.wait()
     for ring in (xr, pr, *wr, *gr):
         ring.finish()

time: 99.1 us -> 96.3 us (0.972)
  Pallas kernels: 98.3 us -> 95.4 us
    pallas_call x1, Pallas kernels: 96.3 us -> 93.3 us  [per_device(): pl.pallas_call(functools.partial(kernel, nz), out_shape=(jax.ShapeDtypeSt...]
where the time goes in v3:
time: 96.3 us; the launch traced here: 96.2 us
  Pallas kernels  95.4 us (99%)
    pallas_call x1, Pallas kernels, per_device(): pl.pallas_call(functools.partial(kernel, nz), out_shape=(jax.ShapeDtypeSt...  93.3 us
    pallas_call x1, Pallas kernels, per_device(): pl.pallas_call(hand_out, out_shape=(jax.ShapeDtypeStruct((per, batch), bf...  2.07 us

profile of v3, /device:TPU:69, one launch (start us, length us, event | category | flops | bytes accessed | tf_op | source)
XLA Modules:
  0.0 96.2 jit_solution(9543631361935839641)
XLA Ops:
  0.6 93.3 %shard_map.131 = (bf16[64,1024]{1,0:T(8,128)(2,1)}, f32[2,2,64,1024]{3,2,1,0:T(8,128)}) custom-call(bf16[64,1024]{1,0:T(8,128)(2,1)} %bitcast.16, f32[2,2,64,1024]{3,2,1,0:T(8,128)} %bitcast.15, bf16[2,16,2048]{2,1,0:T(8,128)(2,1)} %bitcast.17, bf16[2,16,2048]{2,1,0:T(8,128)(2,1)} %bitcast.18, bf16[2,64,512]{2,1,0:T(8,128)(2,1)} %bitcast.19, ...), custom_call_target="tpu_custom_call" | custom-call | tf_op jit(solution)/shard_map/pallas_call | solution.py:514
  93.9 2.1 %shard_map.132 = (bf16[64,1024]{1,0:T(8,128)(2,1)}, f32[2,2,64,1024]{3,2,1,0:T(8,128)}) custom-call(bf16[64,1024]{1,0:T(8,128)(2,1)} %get-tuple-element.6.out_in, f32[2,2,64,1024]{3,2,1,0:T(8,128)} %get-tuple-element.7.fresh_in), custom_call_target="tpu_custom_call" | custom-call | tf_op jit(solution)/shard_map/pallas_call | solution.py:579
